TPU v7x, 32 devices: a whole 2x2x4 slice. The times are simulated.
32 devices in a mesh: rep: 2 (over x), fs: 4 (over z), tp: 4 (over y, core).
Axes of the slice: x: 2, y: 2, z: 4, core: 2. Of those that a mesh axis runs over, the one named last changes fastest.
Arguments:
- tokens: bfloat16 [4096, 2048], P(('rep', 'fs', 'tp')), may hold values from -6 to 6
- mix_gain: bfloat16 [2048], replicated, may hold values from 0.099609375 to 1.8984375
- gate_proj: bfloat16 [2048, 512], P('fs', 'tp'), may hold values from -0.125 to 0.125
- value_proj: bfloat16 [2048, 512], P('fs', 'tp'), may hold values from -1 to 1
- layer_gain: bfloat16 [512], replicated, may hold values from 0.099609375 to 1.8984375
- layer_shift: bfloat16 [512], replicated, may hold values from -3 to 3
- mix_kernel: bfloat16 [4, 128, 128], replicated, may hold values from -0.5 to 0.5
- mix_offset: bfloat16 [4, 128], replicated, may hold values from -4 to 4
- out_proj: bfloat16 [2048, 512], P('fs', 'tp'), may hold values from -0.25 to 0.25
- ffn_gain: bfloat16 [2048], replicated, may hold values from 0.099609375 to 1.8984375
- ffn_gate: bfloat16 [2048, 5632], P('fs', 'tp'), may hold values from -0.125 to 0.125
- ffn_up: bfloat16 [2048, 5632], P('fs', 'tp'), may hold values from -0.125 to 0.125
- ffn_down: bfloat16 [2048, 5632], P('fs', 'tp'), may hold values from -0.078125 to 0.078125
Outputs:
- layer_out: bfloat16 [4096, 2048], P(('rep', 'fs', 'tp'))
All inputs are finite; a program needn't handle non-finite values.
Results may differ from a plain program's by a relative error of at most 0.015.
Values may be sent and summed in bfloat16 or wider, within the bound.
A program may use at most 64 MiB of HBM per device.

v0:
```python
import jax
import jax.numpy as jnp
from jax import lax
from jax.sharding import PartitionSpec as P

epsilon = 1e-06


def rms_norm(rows, gain):
    floats = rows.astype(jnp.float32)
    scale = lax.rsqrt(jnp.mean(floats * floats, axis=-1, keepdims=True) + epsilon)
    return (floats * scale * gain.astype(jnp.float32)).astype(jnp.bfloat16)


def contract_last(left, right):
    return lax.dot_general(
        left, right, (((1,), (1,)), ((), ())), preferred_element_type=jnp.float32
    )


def per_device(
    tokens,
    mix_gain,
    gate_proj,
    value_proj,
    layer_gain,
    layer_shift,
    mix_kernel,
    mix_offset,
    out_proj,
    ffn_gain,
    ffn_gate,
    ffn_up,
    ffn_down,
):
    normed = rms_norm(tokens, mix_gain)
    gate_rows, value_rows, out_rows = (
        lax.all_gather(gate_proj, "fs", axis=0, tiled=True),
        lax.all_gather(value_proj, "fs", axis=0, tiled=True),
        lax.all_gather(out_proj, "fs", axis=0, tiled=True),
    )
    mix_width = layer_gain.shape[0]
    groups = mix_kernel.shape[0]
    span_len = mix_kernel.shape[1]
    causal = jnp.tril(jnp.ones((span_len, span_len), dtype=bool))
    masked = jnp.where(causal[None], mix_kernel, jnp.zeros_like(mix_kernel))
    local_width = gate_rows.shape[1]
    first_col = lax.axis_index("tp") * local_width
    joined = jnp.concatenate([gate_rows, value_rows], axis=1)
    preact = jnp.dot(
        lax.all_gather(normed, "tp", axis=0, tiled=True), joined, preferred_element_type=jnp.float32
    )
    gate_u = jax.nn.gelu(preact[:, :local_width])
    activated = jax.nn.gelu(preact[:, local_width:])
    row_sum, squares = lax.psum(
        (jnp.sum(activated, axis=-1), jnp.sum(activated * activated, axis=-1)), "tp"
    )
    center = (row_sum / mix_width)[:, None]
    spread = (squares / mix_width)[:, None] - center * center
    gain_part = lax.dynamic_slice_in_dim(layer_gain, first_col, local_width).astype(jnp.float32)
    shift_part = lax.dynamic_slice_in_dim(layer_shift, first_col, local_width).astype(jnp.float32)
    values = ((activated - center) * lax.rsqrt(spread + epsilon) * gain_part + shift_part).astype(
        jnp.bfloat16
    )
    group_id = first_col // (mix_width // groups)
    kernel = lax.dynamic_index_in_dim(masked, group_id, 0, keepdims=False)
    offset = lax.dynamic_index_in_dim(mix_offset, group_id, 0, keepdims=False).astype(jnp.float32)
    mixing = jnp.einsum(
        "ts,nsc->ntc",
        kernel,
        values.reshape(-1, span_len, local_width),
        preferred_element_type=jnp.float32,
    )
    mixing = mixing + offset[None, :, None]
    gated_rows = (gate_u * mixing.reshape(gate_u.shape)).astype(jnp.bfloat16)
    mixer_out = lax.psum_scatter(
        contract_last(gated_rows, out_rows).astype(jnp.bfloat16),
        "tp",
        scatter_dimension=0,
        tiled=True,
    ).astype(jnp.float32)
    middle = (tokens.astype(jnp.float32) + mixer_out).astype(jnp.bfloat16)
    normed2 = rms_norm(middle, ffn_gain)
    gathered = lax.all_gather(normed2, "tp", axis=0, tiled=True)
    gate_pre = jnp.dot(
        gathered,
        lax.all_gather(ffn_gate, "fs", axis=0, tiled=True),
        preferred_element_type=jnp.float32,
    )
    up_pre = jnp.dot(
        gathered,
        lax.all_gather(ffn_up, "fs", axis=0, tiled=True),
        preferred_element_type=jnp.float32,
    )
    hidden = (jax.nn.silu(gate_pre) * up_pre).astype(jnp.bfloat16)
    partial_value = contract_last(hidden, lax.all_gather(ffn_down, "fs", axis=0, tiled=True))
    summed = lax.psum_scatter(
        partial_value.astype(jnp.bfloat16), "tp", scatter_dimension=0, tiled=True
    ).astype(jnp.float32)
    return (middle.astype(jnp.float32) + summed).astype(jnp.bfloat16)


def solution(mesh):
    placed = (
        P(("rep", "fs", "tp"), None),
        P(),
        P("fs", "tp"),
        P("fs", "tp"),
        P(),
        P(),
        P(),
        P(),
        P("fs", "tp"),
        P(),
        P("fs", "tp"),
        P("fs", "tp"),
        P("fs", "tp"),
    )
    return jax.shard_map(
        per_device,
        mesh=mesh,
        in_specs=placed,
        out_specs=P(("rep", "fs", "tp"), None),
        check_vma=False,
    )
```

profile of v0, /device:TPU:0, one launch (start us, length us, event | category | flops | bytes accessed | tf_op | source)
XLA Modules:
  0.0 472.7 jit_solution(3375747574779029369)
XLA Ops:
  7.4 0.0 all-gather.6.cloned.1.call-start
  7.4 0.7 convert_element_type.64
  8.1 1.2 fusion.1
  9.3 2.0 fusion.3
  11.4 0.0 all-gather.6.cloned.1.call-update
  11.4 0.0 reduce-scatter.3.cloned.1.call-start
  11.5 0.7 bitcast_convert_fusion
  12.2 0.8 dynamic-slice_convert_fusion
  12.9 17.6 %all_gather.25 = bf16[2048,128]{1,0:T(8,128)(2,1)S(1)} all-gather(bf16[512,128]{1,0:T(8,128)(2,1)} %param.15), channel_id=1, replica_groups=mesh['rep'=2,'fs'=4,'tp'=4] {'fs'}, dimensions={0}, use_global_device_ids=true | all-gather | bytes 655360 | tf_op jit(solution)/shard_map/all_gather | solution.py:38
  30.5 0.0 copy-done.2
  30.5 16.7 %all_gather.26 = bf16[2048,128]{1,0:T(8,128)(2,1)S(1)} all-gather(bf16[512,128]{1,0:T(8,128)(2,1)S(1)} %copy-done.2), channel_id=1, replica_groups=mesh['rep'=2,'fs'=4,'tp'=4] {'fs'}, dimensions={0}, use_global_device_ids=true | all-gather | bytes 655360 | tf_op jit(solution)/shard_map/all_gather | solution.py:39
  47.2 0.0 copy-done.3
  47.2 15.6 %all_gather.27 = bf16[2048,128]{1,0:T(8,128)(2,1)S(1)} all-gather(bf16[512,128]{1,0:T(8,128)(2,1)S(1)} %copy-done.3), channel_id=1, replica_groups=mesh['rep'=2,'fs'=4,'tp'=4] {'fs'}, dimensions={0}, use_global_device_ids=true | all-gather | bytes 655360 | tf_op jit(solution)/shard_map/all_gather | solution.py:40
  62.8 2.3 fusion.9
  65.2 0.2 fusion.37
  65.4 5.7 %all-reduce = (f32[512]{0:T(512)S(1)}, f32[512]{0:T(512)S(1)}) all-reduce(f32[512]{0:T(512)S(1)} %get-tuple-element.6, f32[512]{0:T(512)S(1)} %get-tuple-element.5), channel_id=1, replica_groups=mesh['rep'=2,'fs'=4,'tp'=4] {'tp'}, use_global_device_ids=true, to_apply=%region_4.5 | all-reduce | flops 1024 | bytes 8192 | tf_op jit(solution)/shard_map/psum | solution.py:55
  71.1 0.2 add_convert_fusion
  71.3 0.9 convolution_add_fusion
  72.2 0.1 fusion.21
  72.3 0.0 copy-start.4
  72.4 0.0 copy-start
  72.4 2.1 convolution_convert_fusion
  74.4 0.0 reduce-scatter.3.cloned.1.call-update
  74.5 0.0 all-gather.10.cloned.1.call-start
  74.5 0.5 all-gather.10.cloned.1.call-update
  75.0 0.0 all-gather.8.cloned.1.call-start
  75.1 0.0 copy-done.4
  75.1 31.4 %reduce-scatter.3.cloned.1.call-done = bf16[128,2048]{1,0:T(8,128)(2,1)} async-done(((bf16[512,2048]{1,0:T(8,128)(2,1)}), bf16[128,2048]{1,0:T(8,128)(2,1)}) %reduce-scatter.3.cloned.1.call-update) | async-done | bytes 524304 | tf_op jit(solution)/shard_map/reduce_scatter | solution.py:76
  106.5 0.0 copy-done
  106.5 1.3 fusion.5
  107.8 2.0 fusion.7
  109.9 0.0 all-gather.8.cloned.1.call-update
  109.9 0.0 all-gather.12.cloned.1.call-start
  110.0 0.5 all-gather.12.cloned.1.call-update
  110.5 0.0 all-gather.14.cloned.1.call-start
  110.6 0.7 all-gather.14.cloned.1.call-update
  111.2 0.0 reduce-scatter.5.cloned.1.call-start
  111.3 72.6 %all-gather.10.cloned.1.call-done = bf16[2048,1408]{1,0:T(8,128)(2,1)} async-done(((bf16[512,1408]{1,0:T(8,128)(2,1)}), bf16[2048,1408]{1,0:T(8,128)(2,1)}) %all-gather.10.cloned.1.call-update) | async-done | bytes 5767184 | tf_op jit(solution)/shard_map/all_gather | solution.py:87
  183.9 22.1 %all-gather.8.cloned.1.call-done = bf16[512,2048]{1,0:T(8,128)(2,1)} async-done(((bf16[128,2048]{1,0:T(8,128)(2,1)}), bf16[512,2048]{1,0:T(8,128)(2,1)}) %all-gather.8.cloned.1.call-update) | async-done | bytes 2097168 | tf_op jit(solution)/shard_map/all_gather | solution.py:84
  206.0 8.4 %fusion.38 = f32[512,1408]{1,0:T(8,128)} fusion(bf16[512,2048]{1,0:T(8,128)(2,1)} %all-gather.8.cloned.1.call-done, bf16[2048,1408]{1,0:T(8,128)(2,1)} %all-gather.10.cloned.1.call-done), kind=kOutput, calls=%fused_computation.60 | convolution fusion | flops 2952790016 | bytes 10747904 | tf_op jit(solution)/shard_map/dot_general | solution.py:85
  214.4 99.6 %all-gather.12.cloned.1.call-done = bf16[2048,1408]{1,0:T(8,128)(2,1)} async-done(((bf16[512,1408]{1,0:T(8,128)(2,1)}), bf16[2048,1408]{1,0:T(8,128)(2,1)}) %all-gather.12.cloned.1.call-update) | async-done | bytes 5767184 | tf_op jit(solution)/shard_map/all_gather | solution.py:92
  314.0 106.4 %all-gather.14.cloned.1.call-done = bf16[2048,1408]{1,0:T(8,128)(2,1)} async-done(((bf16[512,1408]{1,0:T(8,128)(2,1)}), bf16[2048,1408]{1,0:T(8,128)(2,1)}) %all-gather.14.cloned.1.call-update) | async-done | bytes 5767184 | tf_op jit(solution)/shard_map/all_gather | solution.py:96
  420.5 0.0 copy-done.5
  420.5 13.2 %convolution_convert_fusion.1 = bf16[512,2048]{1,0:T(8,128)(2,1)} fusion(bf16[2048,1408]{1,0:T(8,128)(2,1)} %all-gather.14.cloned.1.call-done, bf16[512,2048]{1,0:T(8,128)(2,1)S(1)} %copy-done.5, bf16[2048,1408]{1,0:T(8,128)(2,1)} %all-gather.12.cloned.1.call-done, f32[512,1408]{1,0:T(8,128)} %fusion.38), kind=kOutput, calls=%fused_computation.3 | convolution fusion | flops 5910953984 | bytes 18612224 | tf_op jit(solution)/shard_map/dot_general | solution.py:16
  433.7 0.0 reduce-scatter.5.cloned.1.call-update
  433.7 29.6 %reduce-scatter.5.cloned.1.call-done = bf16[128,2048]{1,0:T(8,128)(2,1)} async-done(((bf16[512,2048]{1,0:T(8,128)(2,1)}), bf16[128,2048]{1,0:T(8,128)(2,1)}) %reduce-scatter.5.cloned.1.call-update) | async-done | bytes 524304 | tf_op jit(solution)/shard_map/reduce_scatter | solution.py:97
  463.3 0.0 copy-done.1
  463.3 2.1 fusion.8
  (10 shorter events, 0.1 us)
Async XLA Ops:
  7.4 23.2 %copy-start.2 = (bf16[512,128]{1,0:T(8,128)(2,1)S(1)}, bf16[512,128]{1,0:T(8,128)(2,1)}, u32[]{:S(2)}) copy-start(bf16[512,128]{1,0:T(8,128)(2,1)} %param.16) | copy-start | bytes 393220
  7.4 39.9 %copy-start.3 = (bf16[512,128]{1,0:T(8,128)(2,1)S(1)}, bf16[512,128]{1,0:T(8,128)(2,1)}, u32[]{:S(2)}) copy-start(bf16[512,128]{1,0:T(8,128)(2,1)} %param.21) | copy-start | bytes 393220
  7.4 55.5 %all-gather.6.cloned.1.call-start = ((), (), s32[]{:S(2)}) async-start(), calls=%async_computation.2 | async-start | bytes 2621440 | tf_op jit(solution)/shard_map/all_gather | solution.py:51
  11.4 95.1 %reduce-scatter.3.cloned.1.call-start = ((), (), s32[]{:S(2)}) async-start(), calls=%async_computation.3 | async-start | bytes 2621440 | tf_op jit(solution)/shard_map/reduce_scatter | solution.py:76
  72.3 2.7 copy-start.4
  72.4 34.2 %copy-start = (bf16[128,2048]{1,0:T(8,128)(2,1)S(1)}, bf16[128,2048]{1,0:T(8,128)(2,1)}, u32[]{:S(2)}) copy-start(bf16[128,2048]{1,0:T(8,128)(2,1)} %param.13) | copy-start | bytes 1572868
  74.5 109.4 %all-gather.10.cloned.1.call-start = ((), (), s32[]{:S(2)}) async-start(), calls=%async_computation.5 | async-start | bytes 7208960 | tf_op jit(solution)/shard_map/all_gather | solution.py:87
  75.0 131.0 %all-gather.8.cloned.1.call-start = ((), (), s32[]{:S(2)}) async-start(), calls=%async_computation.4 | async-start | bytes 2621440 | tf_op jit(solution)/shard_map/all_gather | solution.py:84
  109.9 204.1 %all-gather.12.cloned.1.call-start = ((), (), s32[]{:S(2)}) async-start(), calls=%async_computation.6 | async-start | bytes 7208960 | tf_op jit(solution)/shard_map/all_gather | solution.py:92
  110.5 310.0 %all-gather.14.cloned.1.call-start = ((), (), s32[]{:S(2)}) async-start(), calls=%async_computation.7 | async-start | bytes 7208960 | tf_op jit(solution)/shard_map/all_gather | solution.py:96
  111.2 352.1 %reduce-scatter.5.cloned.1.call-start = ((), (), s32[]{:S(2)}) async-start(), calls=%async_computation.8 | async-start | bytes 2621440 | tf_op jit(solution)/shard_map/reduce_scatter | solution.py:97
  206.0 214.5 %copy-start.5 = (bf16[512,2048]{1,0:T(8,128)(2,1)S(1)}, bf16[512,2048]{1,0:T(8,128)(2,1)}, u32[]{:S(2)}) copy-start(bf16[512,2048]{1,0:T(8,128)(2,1)} %all-gather.8.cloned.1.call-done) | copy-start | bytes 6291460
  214.4 248.9 %copy-start.1 = (bf16[128,2048]{1,0:T(8,128)(2,1)S(1)}, bf16[128,2048]{1,0:T(8,128)(2,1)}, u32[]{:S(2)}) copy-start(bf16[128,2048]{1,0:T(8,128)(2,1)} %reduce-scatter.3.cloned.1.call-done) | copy-start | bytes 1572868
Sparse Core Ops, SparseCore 0:
  11.5 25.2 all-gather.5
  74.6 31.9 reduce-scatter.2
  433.8 29.4 reduce-scatter.4
Sparse Core Ops, SparseCore 1:
  76.5 107.3 all-gather.9
  185.3 20.7 all-gather.7
  207.5 106.5 all-gather.11
  315.6 104.8 all-gather.13
where the time goes:
time: 473 us
  waiting for transfers between devices  364 us (77%)
  blocking collectives  55.5 us (12%)
  matrix products  26.9 us (6%)
  between operations  14.9 us (3%)
  other arithmetic  11.5 us (2%)
    all_gather x1, waiting for transfers between devices, per_device(): lax.all_gather(ffn_down, 'fs', axis=0, tiled=True)  106 us
    all_gather x1, waiting for transfers between devices, per_device(): lax.all_gather(ffn_up, 'fs', axis=0, tiled=True)  99.6 us
    all_gather x1, waiting for transfers between devices, per_device(): lax.all_gather(ffn_gate, 'fs', axis=0, tiled=True)  72.6 us
    reduce_scatter x1, waiting for transfers between devices, per_device(): lax.psum_scatter(contract_last(gated_rows, out_rows).astype(jnp.bfloat16)...  31.4 us
    reduce_scatter x1, waiting for transfers between devices, per_device(): lax.psum_scatter(partial_value.astype(jnp.bfloat16), 'tp', scatter_dimens...  29.6 us
    all_gather x1, waiting for transfers between devices, per_device(): gathered = lax.all_gather(normed2, 'tp', axis=0, tiled=True)  22.1 us
    all_gather x1, blocking collectives, per_device(): lax.all_gather(gate_proj, 'fs', axis=0, tiled=True)  17.6 us
    all_gather x1, blocking collectives, per_device(): lax.all_gather(value_proj, 'fs', axis=0, tiled=True)  16.7 us
  transfers between devices with their start and end apart: 7, of which 6 were waited for; matrix products, arithmetic and copies ran while one was open for 3% of the time, Pallas kernels for 0%

commit v1 on v0

--- a/solution.py
+++ b/solution.py
@@ -4,6 +4,19 @@
 from jax.sharding import PartitionSpec as P
 
 epsilon = 1e-06
+
+
+def ring_gather(x, axis, dim):
+    ways = lax.axis_size(axis)
+    up = [(d, (d + 1) % ways) for d in range(ways)]
+    down = [(d, (d - 1) % ways) for d in range(ways)]
+    earlier, later = ([x], [x])
+    for _ in range(ways // 2):
+        earlier.append(lax.ppermute(earlier[-1], axis, up))
+    for _ in range((ways - 1) // 2):
+        later.append(lax.ppermute(later[-1], axis, down))
+    line = jnp.concatenate([*earlier[::-1], *later[1:]], axis=dim)
+    return jnp.roll(line, (lax.axis_index(axis) - ways // 2) * x.shape[dim], axis=dim)
 
 
 def rms_norm(rows, gain):
@@ -87,11 +100,7 @@
         lax.all_gather(ffn_gate, "fs", axis=0, tiled=True),
         preferred_element_type=jnp.float32,
     )
-    up_pre = jnp.dot(
-        gathered,
-        lax.all_gather(ffn_up, "fs", axis=0, tiled=True),
-        preferred_element_type=jnp.float32,
-    )
+    up_pre = jnp.dot(gathered, ring_gather(ffn_up, "fs", 0), preferred_element_type=jnp.float32)
     hidden = (jax.nn.silu(gate_pre) * up_pre).astype(jnp.bfloat16)
     partial_value = contract_last(hidden, lax.all_gather(ffn_down, "fs", axis=0, tiled=True))
     summed = lax.psum_scatter(

time: 473 us -> 432 us (0.913)
  waiting for transfers between devices: 364 us -> 272 us
  starting transfers between devices: 0.26 us -> 34.9 us
  local copies, waits for them, and re-layouts: 0.03 us -> 15.6 us
    ppermute x0 -> x3, waiting for transfers between devices: none -> 124 us  [the longest x2 101 us: ring_gather(): earlier.append(lax.ppermute(earlier[-1], axis, up))]
    all_gather x1 -> x0, waiting for transfers between devices: 99.6 us -> none  [per_device(): lax.all_gather(ffn_up, 'fs', axis=0, tiled=True)]
    all_gather x1, waiting for transfers between devices: 72.6 us -> 0.01 us  [per_device(): lax.all_gather(ffn_gate, 'fs', axis=0, tiled=True)]
    ppermute x0 -> x3, starting transfers between devices: none -> 34.6 us  [the longest x2 28.4 us: ring_gather(): earlier.append(lax.ppermute(earlier[-1], axis, up))]
    all_gather x1, waiting for transfers between devices: 22.1 us -> 0.01 us  [per_device(): gathered = lax.all_gather(normed2, 'tp', axis=0, tiled=True)]
    all_gather x1, waiting for transfers between devices: 106 us -> 86.2 us  [per_device(): lax.all_gather(ffn_down, 'fs', axis=0, tiled=True)]
    unnamed x12 -> x21, local copies, waits for them, and re-layouts: 0.03 us -> 12.9 us
  transfers between devices with their start and end apart: 7 -> 9, of which waited for: 6 -> 6; matrix products, arithmetic and copies ran while one was open for 3% -> 7% of each run, Pallas kernels for 0% -> 0%
where the time goes in v1:
time: 432 us
  waiting for transfers between devices  272 us (63%)
  blocking collectives  55.5 us (13%)
  starting transfers between devices  34.9 us (8%)
  matrix products  27 us (6%)
  local copies, waits for them, and re-layouts  15.6 us (4%)
  between operations  14.9 us (3%)
  other arithmetic  11.5 us (3%)
    ppermute x2, waiting for transfers between devices, ring_gather(): earlier.append(lax.ppermute(earlier[-1], axis, up))  101 us
    all_gather x1, waiting for transfers between devices, per_device(): lax.all_gather(ffn_down, 'fs', axis=0, tiled=True)  86.2 us
    reduce_scatter x1, waiting for transfers between devices, per_device(): lax.psum_scatter(contract_last(gated_rows, out_rows).astype(jnp.bfloat16)...  31.4 us
    reduce_scatter x1, waiting for transfers between devices, per_device(): lax.psum_scatter(partial_value.astype(jnp.bfloat16), 'tp', scatter_dimens...  29.6 us
    ppermute x2, starting transfers between devices, ring_gather(): earlier.append(lax.ppermute(earlier[-1], axis, up))  28.4 us
    ppermute x1, waiting for transfers between devices, ring_gather(): later.append(lax.ppermute(later[-1], axis, down))  23.1 us
    all_gather x1, blocking collectives, per_device(): lax.all_gather(gate_proj, 'fs', axis=0, tiled=True)  17.6 us
    all_gather x1, blocking collectives, per_device(): lax.all_gather(value_proj, 'fs', axis=0, tiled=True)  16.7 us
  transfers between devices with their start and end apart: 9, of which 6 were waited for; matrix products, arithmetic and copies ran while one was open for 7% of the time, Pallas kernels for 0%

profile of v1, /device:TPU:0, one launch (start us, length us, event | category | flops | bytes accessed | tf_op | source)
XLA Modules:
  0.0 431.5 jit_solution(6863769381710729109)
XLA Ops:
  7.4 0.7 convert_element_type.64
  8.1 1.2 fusion.8
  9.3 2.0 fusion.10
  11.4 0.0 all-gather.5.cloned.1.call-update
  11.4 0.0 reduce-scatter.3.cloned.1.call-start
  11.5 0.7 fusion.46
  12.2 0.8 dynamic-slice_convert_fusion
  12.9 17.6 %all_gather.22 = bf16[2048,128]{1,0:T(8,128)(2,1)S(1)} all-gather(bf16[512,128]{1,0:T(8,128)(2,1)} %param.15), channel_id=1, replica_groups=mesh['rep'=2,'fs'=4,'tp'=4] {'fs'}, dimensions={0}, use_global_device_ids=true | all-gather | bytes 655360 | tf_op jit(solution)/shard_map/all_gather | solution.py:51
  30.5 16.7 %all_gather.23 = bf16[2048,128]{1,0:T(8,128)(2,1)S(1)} all-gather(bf16[512,128]{1,0:T(8,128)(2,1)S(1)} %copy-done.3), channel_id=1, replica_groups=mesh['rep'=2,'fs'=4,'tp'=4] {'fs'}, dimensions={0}, use_global_device_ids=true | all-gather | bytes 655360 | tf_op jit(solution)/shard_map/all_gather | solution.py:52
  47.2 15.6 %all_gather.24 = bf16[2048,128]{1,0:T(8,128)(2,1)S(1)} all-gather(bf16[512,128]{1,0:T(8,128)(2,1)S(1)} %copy-done.4), channel_id=1, replica_groups=mesh['rep'=2,'fs'=4,'tp'=4] {'fs'}, dimensions={0}, use_global_device_ids=true | all-gather | bytes 655360 | tf_op jit(solution)/shard_map/all_gather | solution.py:53
  62.8 2.3 fusion.16
  65.1 0.2 fusion.50
  65.4 5.7 %all-reduce = (f32[512]{0:T(512)S(1)}, f32[512]{0:T(512)S(1)}) all-reduce(f32[512]{0:T(512)S(1)} %get-tuple-element.6, f32[512]{0:T(512)S(1)} %get-tuple-element.5), channel_id=1, replica_groups=mesh['rep'=2,'fs'=4,'tp'=4] {'tp'}, use_global_device_ids=true, to_apply=%region_4.5 | all-reduce | flops 1024 | bytes 8192 | tf_op jit(solution)/shard_map/psum | solution.py:68
  71.1 0.2 add_convert_fusion
  71.3 0.9 convolution_add_fusion
  72.2 0.1 fusion.30
  72.4 2.0 convolution_convert_fusion
  74.4 0.0 reduce-scatter.3.cloned.1.call-update
  74.4 0.0 all-gather.9.cloned.1.call-start
  74.5 0.5 all-gather.9.cloned.1.call-update
  75.0 0.0 all-gather.7.cloned.1.call-start
  75.1 31.4 %reduce-scatter.3.cloned.1.call-done = bf16[128,2048]{1,0:T(8,128)(2,1)} async-done(((bf16[512,2048]{1,0:T(8,128)(2,1)}), bf16[128,2048]{1,0:T(8,128)(2,1)}) %reduce-scatter.3.cloned.1.call-update) | async-done | bytes 524304 | tf_op jit(solution)/shard_map/reduce_scatter | solution.py:89
  106.5 1.3 fusion.12
  107.8 2.0 fusion.14
  109.9 0.0 all-gather.7.cloned.1.call-update
  109.9 0.0 all-gather.11.cloned.1.call-start
  109.9 0.5 all-gather.11.cloned.1.call-update
  110.5 0.0 reduce-scatter.5.cloned.1.call-start
  110.5 1.5 collective-permute-start
  112.1 65.3 %collective-permute-done = bf16[512,1408]{1,0:T(8,128)(2,1)S(1)} collective-permute-done((bf16[512,1408]{1,0:T(8,128)(2,1)S(1)}, bf16[512,1408]{1,0:T(8,128)(2,1)S(1)}, u32[]{:S(2)}, u32[]{:S(2)}) %collective-permute-start) | collective-permute-done | bytes 1441824 | tf_op jit(solution)/shard_map/ppermute | solution.py:15
  177.4 26.8 %collective-permute-start.1 = (bf16[512,1408]{1,0:T(8,128)(2,1)S(1)}, bf16[512,1408]{1,0:T(8,128)(2,1)}, u32[]{:S(2)}, u32[]{:S(2)}) collective-permute-start(bf16[512,1408]{1,0:T(8,128)(2,1)S(1)} %collective-permute-done), channel_id=1, source_target_pairs={{0,4},{4,8},{8,12},{12,0},{1,5},{5,9},{9,13},{13,1},{2,6},{6,10},{... | collective-permute-start | bytes 4325384 | tf_op jit(solution)/shard_map/ppermute | solution.py:15
  204.2 6.3 %collective-permute-start.2 = (bf16[512,1408]{1,0:T(8,128)(2,1)S(1)}, bf16[512,1408]{1,0:T(8,128)(2,1)}, u32[]{:S(2)}, u32[]{:S(2)}) collective-permute-start(bf16[512,1408]{1,0:T(8,128)(2,1)S(1)} %copy-done.1), channel_id=1, source_target_pairs={{0,12},{4,0},{8,4},{12,8},{1,13},{5,1},{9,5},{13,9},{2,14},{6,2},{... | collective-permute-start | bytes 4325384 | tf_op jit(solution)/shard_map/ppermute | solution.py:17
  210.5 35.5 %collective-permute-done.1 = bf16[512,1408]{1,0:T(8,128)(2,1)} collective-permute-done((bf16[512,1408]{1,0:T(8,128)(2,1)S(1)}, bf16[512,1408]{1,0:T(8,128)(2,1)}, u32[]{:S(2)}, u32[]{:S(2)}) %collective-permute-start.1) | collective-permute-done | bytes 1441824 | tf_op jit(solution)/shard_map/ppermute | solution.py:15
  246.0 2.6 constant_dynamic-update-slice_fusion.7
  248.6 1.2 constant_dynamic-update-slice_fusion.6
  249.8 1.2 constant_dynamic-update-slice_fusion.5
  251.0 23.1 %collective-permute-done.2 = bf16[512,1408]{1,0:T(8,128)(2,1)} collective-permute-done((bf16[512,1408]{1,0:T(8,128)(2,1)S(1)}, bf16[512,1408]{1,0:T(8,128)(2,1)}, u32[]{:S(2)}, u32[]{:S(2)}) %collective-permute-start.2) | collective-permute-done | bytes 1441824 | tf_op jit(solution)/shard_map/ppermute | solution.py:17
  274.1 2.6 constant_dynamic-update-slice_fusion.4
  276.7 2.6 constant_dynamic-update-slice_fusion.3
  279.3 1.3 constant_dynamic-update-slice_fusion.2
  280.6 1.3 constant_dynamic-update-slice_fusion.1
  281.9 2.7 constant_dynamic-update-slice_fusion
  284.6 8.4 %fusion.51 = f32[512,1408]{1,0:T(8,128)} fusion(bf16[512,2048]{1,0:T(8,128)(2,1)} %all-gather.7.cloned.1.call-done, bf16[2048,1408]{1,0:T(8,128)(2,1)} %all-gather.9.cloned.1.call-done), kind=kOutput, calls=%fused_computation.73 | convolution fusion | flops 2952790016 | bytes 10747904 | tf_op jit(solution)/shard_map/dot_general | solution.py:98
  293.0 86.2 %all-gather.11.cloned.1.call-done = bf16[2048,1408]{1,0:T(8,128)(2,1)} async-done(((bf16[512,1408]{1,0:T(8,128)(2,1)}), bf16[2048,1408]{1,0:T(8,128)(2,1)}) %all-gather.11.cloned.1.call-update) | async-done | bytes 5767184 | tf_op jit(solution)/shard_map/all_gather | solution.py:105
  379.2 13.3 %convolution_convert_fusion.1 = bf16[512,2048]{1,0:T(8,128)(2,1)} fusion(bf16[2048,1408]{1,0:T(8,128)(2,1)} %all-gather.11.cloned.1.call-done, bf16[512,2048]{1,0:T(8,128)(2,1)S(1)} %copy-done.6, bf16[4096,1408]{1,0:T(8,128)(2,1)} %constant_dynamic-update-slice_fusion, s32[]{:T(128)S(6)} %select_n.38, f32[512,1408]{1,0:T(8,128)} %fusion.51), kind=kOutput, calls=%fused_computation.5 | convolution fusion | flops 5910953984 | bytes 18612228 | tf_op jit(solution)/shard_map/dot_general | solution.py:29
  392.5 0.0 reduce-scatter.5.cloned.1.call-update
  392.5 29.6 %reduce-scatter.5.cloned.1.call-done = bf16[128,2048]{1,0:T(8,128)(2,1)} async-done(((bf16[512,2048]{1,0:T(8,128)(2,1)}), bf16[128,2048]{1,0:T(8,128)(2,1)}) %reduce-scatter.5.cloned.1.call-update) | async-done | bytes 524304 | tf_op jit(solution)/shard_map/reduce_scatter | solution.py:106
  422.1 2.1 fusion.15
  (23 shorter events, 0.1 us)
Async XLA Ops:
  7.4 23.2 %copy-start.3 = (bf16[512,128]{1,0:T(8,128)(2,1)S(1)}, bf16[512,128]{1,0:T(8,128)(2,1)}, u32[]{:S(2)}) copy-start(bf16[512,128]{1,0:T(8,128)(2,1)} %param.16) | copy-start | bytes 393220
  7.4 39.9 %copy-start.4 = (bf16[512,128]{1,0:T(8,128)(2,1)S(1)}, bf16[512,128]{1,0:T(8,128)(2,1)}, u32[]{:S(2)}) copy-start(bf16[512,128]{1,0:T(8,128)(2,1)} %param.21) | copy-start | bytes 393220
  7.4 55.5 %all-gather.5.cloned.1.call-start = ((), (), s32[]{:S(2)}) async-start(), calls=%async_computation.2 | async-start | bytes 2621440 | tf_op jit(solution)/shard_map/all_gather | solution.py:64
  11.4 95.1 %reduce-scatter.3.cloned.1.call-start = ((), (), s32[]{:S(2)}) async-start(), calls=%async_computation.3 | async-start | bytes 2621440 | tf_op jit(solution)/shard_map/reduce_scatter | solution.py:89
  72.3 2.7 copy-start.5
  72.3 34.2 %copy-start = (bf16[128,2048]{1,0:T(8,128)(2,1)S(1)}, bf16[128,2048]{1,0:T(8,128)(2,1)}, u32[]{:S(2)}) copy-start(bf16[128,2048]{1,0:T(8,128)(2,1)} %param.13) | copy-start | bytes 1572868
  74.4 36.1 %copy-start.1 = (bf16[512,1408]{1,0:T(8,128)(2,1)S(1)}, bf16[512,1408]{1,0:T(8,128)(2,1)}, u32[]{:S(2)}) copy-start(bf16[512,1408]{1,0:T(8,128)(2,1)} %param.24) | copy-start | bytes 4325380
  74.4 210.1 %all-gather.9.cloned.1.call-start = ((), (), s32[]{:S(2)}) async-start(), calls=%async_computation.5 | async-start | bytes 7208960 | tf_op jit(solution)/shard_map/all_gather | solution.py:100
  75.0 209.6 %all-gather.7.cloned.1.call-start = ((), (), s32[]{:S(2)}) async-start(), calls=%async_computation.4 | async-start | bytes 2621440 | tf_op jit(solution)/shard_map/all_gather | solution.py:97
  109.9 269.3 %all-gather.11.cloned.1.call-start = ((), (), s32[]{:S(2)}) async-start(), calls=%async_computation.6 | async-start | bytes 7208960 | tf_op jit(solution)/shard_map/all_gather | solution.py:105
  110.5 311.6 %reduce-scatter.5.cloned.1.call-start = ((), (), s32[]{:S(2)}) async-start(), calls=%async_computation.7 | async-start | bytes 2621440 | tf_op jit(solution)/shard_map/reduce_scatter | solution.py:106
  110.5 66.8 %collective-permute-start = (bf16[512,1408]{1,0:T(8,128)(2,1)S(1)}, bf16[512,1408]{1,0:T(8,128)(2,1)S(1)}, u32[]{:S(2)}, u32[]{:S(2)}) collective-permute-start(bf16[512,1408]{1,0:T(8,128)(2,1)S(1)} %copy-done.1), channel_id=1, source_target_pairs={{0,4},{4,8},{8,12},{12,0},{1,5},{5,9},{9,13},{13,1},{2,6},{6,10},{... | collective-permute-start | bytes 4325384 | tf_op jit(solution)/shard_map/ppermute | solution.py:15
  177.4 68.6 %collective-permute-start.1 = (bf16[512,1408]{1,0:T(8,128)(2,1)S(1)}, bf16[512,1408]{1,0:T(8,128)(2,1)}, u32[]{:S(2)}, u32[]{:S(2)}) collective-permute-start(bf16[512,1408]{1,0:T(8,128)(2,1)S(1)} %collective-permute-done), channel_id=1, source_target_pairs={{0,4},{4,8},{8,12},{12,0},{1,5},{5,9},{9,13},{13,1},{2,6},{6,10},{... | collective-permute-start | bytes 4325384 | tf_op jit(solution)/shard_map/ppermute | solution.py:15
  204.2 69.9 %collective-permute-start.2 = (bf16[512,1408]{1,0:T(8,128)(2,1)S(1)}, bf16[512,1408]{1,0:T(8,128)(2,1)}, u32[]{:S(2)}, u32[]{:S(2)}) collective-permute-start(bf16[512,1408]{1,0:T(8,128)(2,1)S(1)} %copy-done.1), channel_id=1, source_target_pairs={{0,12},{4,0},{8,4},{12,8},{1,13},{5,1},{9,5},{13,9},{2,14},{6,2},{... | collective-permute-start | bytes 4325384 | tf_op jit(solution)/shard_map/ppermute | solution.py:17
  284.6 94.6 %copy-start.6 = (bf16[512,2048]{1,0:T(8,128)(2,1)S(1)}, bf16[512,2048]{1,0:T(8,128)(2,1)}, u32[]{:S(2)}) copy-start(bf16[512,2048]{1,0:T(8,128)(2,1)} %all-gather.7.cloned.1.call-done) | copy-start | bytes 6291460
  293.0 129.1 %copy-start.2 = (bf16[128,2048]{1,0:T(8,128)(2,1)S(1)}, bf16[128,2048]{1,0:T(8,128)(2,1)}, u32[]{:S(2)}) copy-start(bf16[128,2048]{1,0:T(8,128)(2,1)} %reduce-scatter.3.cloned.1.call-done) | copy-start | bytes 1572868
Sparse Core Ops, SparseCore 0:
  11.5 25.2 all-gather.4
  74.5 31.9 reduce-scatter.2
  392.6 29.4 reduce-scatter.4
Sparse Core Ops, SparseCore 1:
  76.5 172.2 all-gather.8
  250.2 20.9 all-gather.6
  272.6 106.5 all-gather.10
